TPU v7x, 512 devices: a whole 4x8x8 slice. The times are simulated.
512 devices in a mesh: sp: 32 (over z, x), tp: 16 (over y, core).
Axes of the slice: x: 4, y: 8, z: 8, core: 2. Of those that a mesh axis runs over, the one named last changes fastest.
Arguments:
- ffn_input: bfloat16 [4096, 2048], P('sp', 'tp'), may hold values from -6 to 6
- out_grad: bfloat16 [4096, 2048], P('sp', 'tp'), may hold values from -6 to 6
- routes: int32 [4096, 2], P('sp'), may hold values from 0 to 31, all different within a row; in each aligned block of 128 rows (0 to 127, 128 to 255, ...) at most 10 rows name the same one
- route_weight: float32 [4096, 2], P('sp'), may hold values from 0.05 to 1
- gate_w: bfloat16 [32, 2048, 2048], P('sp', None, 'tp'), may hold values from -0.125 to 0.125
- up_w: bfloat16 [32, 2048, 2048], P('sp', None, 'tp'), may hold values from -0.125 to 0.125
- down_w: bfloat16 [32, 2048, 2048], P('sp', 'tp'), may hold values from -0.125 to 0.125
- out_proj: bfloat16 [2048, 2048], P('tp'), may hold values from -0.125 to 0.125
- rec_value: bfloat16 [4096, 2048], P('sp', 'tp'), may hold values from -6 to 6
- rate_pre: bfloat16 [4096, 2048], P('sp', 'tp'), may hold values from -6 to 6
- input_pre: bfloat16 [4096, 2048], P('sp', 'tp'), may hold values from -4 to 4
- prev_state: bfloat16 [4096, 2048], P('sp', 'tp'), may hold values from -6 to 6
- decay_param: float32 [2048], P('tp'), may hold values from 4 to 12
Outputs:
- gate_w_grad: bfloat16 [32, 2048, 2048], P('sp', None, 'tp')
- up_w_grad: bfloat16 [32, 2048, 2048], P('sp', None, 'tp')
- down_w_grad: bfloat16 [32, 2048, 2048], P('sp', 'tp')
- out_proj_grad: float32 [2048, 2048], P('sp', 'tp')
- rec_value_grad: bfloat16 [4096, 2048], P('sp', 'tp')
- rate_pre_grad: bfloat16 [4096, 2048], P('sp', 'tp')
- input_pre_grad: bfloat16 [4096, 2048], P('sp', 'tp')
Inputs may be any that keep to these rules, and one draw needn't show every extreme that they name: `routes`: each token names 2 different experts. Within each aligned block of 128 tokens no expert is named more than 10 times, a bound that some block reaches.
All inputs are finite; a program needn't handle non-finite values.
Results may differ from a plain program's by a relative error of at most 0.02.
Values may be sent and summed in bfloat16 or wider, within the bound.
A program may use at most 64 MiB of HBM per device.

v0:
```python
import jax
import jax.numpy as jnp
from jax import lax
from jax.sharding import Mesh
from jax.sharding import PartitionSpec as P

SP = ("sp_0", "sp_1")


decay_scale = 8.0


def in_one_piece(arrays, axis, split_dim, concat_dim, along):
    both = jnp.concatenate(arrays, axis=along)
    filled, at, finished = (
        lax.all_to_all(both, axis, split_axis=split_dim, concat_axis=concat_dim, tiled=True),
        0,
        [],
    )
    for a in arrays:
        finished.append(lax.slice_in_dim(filled, at, at + a.shape[along], axis=along))
        at += a.shape[along]
    return tuple(finished)


def sent_together(arrays, axis, dim, along):
    ends, at = ([], 0)
    for a in arrays[:-1]:
        at += a.shape[along]
        ends.append(at)
    both = jnp.concatenate(arrays, axis=along)
    return tuple(jnp.split(lax.all_gather(both, axis, axis=dim, tiled=True), ends, axis=along))


def split_up(shard, dim, length):
    lengths = shard.shape
    tiles = shard.reshape(*lengths[:dim], length, lengths[dim] // length, *lengths[dim + 1 :])
    return jnp.moveaxis(tiles, dim, 0)


def sent_and_summed(shard, axis, dim):
    tiles = split_up(shard, dim, lax.axis_size(axis))
    arrived = lax.all_to_all(tiles, axis, split_axis=0, concat_axis=0, tiled=True)
    return arrived.astype(jnp.float32).sum(axis=0)


def neutral_like(shard, identity):
    return jax.tree.map(
        lambda a, e: jnp.broadcast_to(jnp.asarray(e, a.dtype), a.shape), shard, identity
    )


def all_in_one(shard, axis):
    leaves = jax.tree.leaves(shard)
    sequence = sorted(range(len(leaves)), key=lambda k: -leaves[k].size)
    width = (1, *leaves[sequence[0]].shape)[-1]
    lines = [
        jnp.pad(leaves[k].reshape(-1), (0, -leaves[k].size % width)).reshape(-1, width)
        for k in sequence
    ]
    both, at, found = (lax.all_gather(jnp.concatenate(lines), axis), 0, {})
    for k, line in zip(sequence, lines):
        share = both[:, at : at + len(line)].reshape(len(both), -1)
        found[k] = share[:, : leaves[k].size].reshape(-1, *leaves[k].shape)
        at += len(line)
    numbers = iter(range(len(leaves)))
    return jax.tree.map(lambda _: found[next(numbers)], shard)


def entering(shard, axes, combine, identity):
    before = start = neutral_like(shard, identity)
    so_far = shard
    for axis in reversed(axes):
        length, here = (lax.axis_size(axis), lax.axis_index(axis))
        pieces = all_in_one(so_far, axis)
        inside, so_far = (start, start)
        for k in reversed(range(length)):
            passed = k > here
            so_far = combine(so_far, jax.tree.map(lambda part: part[k], pieces))
            inside = jax.tree.map(lambda new, old: jnp.where(passed, new, old), so_far, inside)
        before = combine(inside, before)
    return before


def chain_link(left_pair, right_pair):
    return (left_pair[0] * right_pair[0], right_pair[0] * left_pair[1] + right_pair[1])


def compose(earlier_map, later_map):
    return (later_map[0] * earlier_map[0], later_map[1] + later_map[0] * earlier_map[1])


def slot_layout(routes, experts, capacity):
    flat_routes = routes.reshape(-1)
    route_marks = (flat_routes[:, None] == jnp.arange(experts, dtype=jnp.int32)[None, :]).astype(
        jnp.int32
    )
    before = jnp.sum((jnp.cumsum(route_marks, axis=0) - route_marks) * route_marks, axis=1)
    slot_index = flat_routes * capacity + before
    slot_total = experts * capacity
    route_ids = jnp.arange(flat_routes.shape[0], dtype=jnp.int32)
    slot_owner = jnp.zeros((slot_total,), jnp.int32).at[slot_index].set(route_ids)
    filled = jnp.zeros((slot_total,), jnp.int32).at[slot_index].set(1)
    return (slot_index, slot_owner, filled)


def fill_slots(tokens_in, cotangent, route_weight, slot_owner, filled, route_count):
    token_index = slot_owner // route_count
    kept_mask = filled[:, None] > 0
    rows_in = jnp.where(
        kept_mask, jnp.take(tokens_in, token_index, axis=0), jnp.zeros((), jnp.bfloat16)
    )
    weights = route_weight.reshape(-1)[slot_owner][:, None]
    scaled = (weights * jnp.take(cotangent, token_index, axis=0).astype(jnp.float32)).astype(
        jnp.bfloat16
    )
    rows_cot = jnp.where(kept_mask, scaled, jnp.zeros((), jnp.bfloat16))
    return (rows_in, rows_cot)


def expert_work(rows_in, rows_cot, w_gate, w_up, w_down):
    across = (((0,), (0,)), ((), ()))
    inner = (((1,), (1,)), ((), ()))
    gate_act = jnp.dot(rows_in, w_gate, preferred_element_type=jnp.float32)
    up_act = jnp.dot(rows_in, w_up, preferred_element_type=jnp.float32)
    squash = jax.nn.sigmoid(gate_act)
    silu_gate = gate_act * squash
    hidden = (silu_gate * up_act).astype(jnp.bfloat16)
    down_grad = lax.dot_general(
        hidden, rows_cot, across, preferred_element_type=jnp.float32
    ).astype(jnp.bfloat16)
    hidden_grad = lax.dot_general(rows_cot, w_down, inner, preferred_element_type=jnp.float32)
    gate_grad = (hidden_grad * up_act * squash * (1.0 + gate_act * (1.0 - squash))).astype(
        jnp.bfloat16
    )
    up_grad = (hidden_grad * silu_gate).astype(jnp.bfloat16)
    gate_w_grad = lax.dot_general(
        rows_in, gate_grad, across, preferred_element_type=jnp.float32
    ).astype(jnp.bfloat16)
    up_w_grad = lax.dot_general(
        rows_in, up_grad, across, preferred_element_type=jnp.float32
    ).astype(jnp.bfloat16)
    row_part = lax.dot_general(gate_grad, w_gate, inner, preferred_element_type=jnp.float32)
    row_part = row_part + lax.dot_general(up_grad, w_up, inner, preferred_element_type=jnp.float32)
    return (gate_w_grad, up_w_grad, down_grad, row_part)


def gather_back(returned, slot_index, cotangent, route_count):
    picked = jnp.take(returned, slot_index, axis=0).astype(jnp.float32)
    summed = jnp.sum(picked.reshape(-1, route_count, picked.shape[1]), axis=1)
    return (summed + cotangent.astype(jnp.float32)).astype(jnp.bfloat16)


def per_device(
    ffn_input,
    out_grad,
    routes,
    route_weight,
    gate_w,
    up_w,
    down_w,
    out_proj,
    rec_value,
    rate_pre,
    input_pre,
    prev_state,
    decay_param,
):
    experts = lax.axis_size(SP)
    tok_rows, route_count = routes.shape
    capacity = 5 * route_count * tok_rows // (4 * experts)
    slot_index, slot_owner, filled = slot_layout(routes, experts, capacity)
    w_gate, w_up, w_down = (gate_w[0], up_w[0], down_w[0])
    send_in, send_cot = fill_slots(
        ffn_input, out_grad, route_weight, slot_owner, filled, route_count
    )
    part_in, part_cot = in_one_piece((send_in, send_cot), SP, 0, 0, 1)
    got_in, got_cot = sent_together((part_in, part_cot), "tp", 1, 0)
    expert_out = expert_work(got_in, got_cot, w_gate, w_up, w_down)
    summed_share = sent_and_summed(expert_out[3].astype(jnp.bfloat16), "tp", 1).astype(jnp.bfloat16)
    returned = lax.all_to_all(summed_share, SP, split_axis=0, concat_axis=0, tiled=True)
    own_grad = gather_back(returned, slot_index, out_grad, route_count)
    mix_grad = lax.all_gather(own_grad, "tp", axis=1, tiled=True)
    state_grad = lax.dot_general(
        mix_grad, out_proj, (((1,), (1,)), ((), ())), preferred_element_type=jnp.float32
    )
    rate_gate = jax.nn.sigmoid(rate_pre.astype(jnp.float32))
    input_gate = jax.nn.sigmoid(input_pre.astype(jnp.float32))
    decay_speed = jax.nn.softplus(-decay_param)[None, :]
    log_decay = -decay_scale * rate_gate * decay_speed
    decay = jnp.exp(log_decay)
    scale_in = jnp.sqrt(-jnp.expm1(2.0 * log_decay))
    signal = rec_value.astype(jnp.float32)
    before_state = prev_state.astype(jnp.float32)
    rec_state = (decay * before_state + scale_in * input_gate * signal).astype(jnp.bfloat16)
    out_proj_grad = sent_and_summed(
        lax.dot_general(
            mix_grad, rec_state, (((0,), (0,)), ((), ())), preferred_element_type=jnp.float32
        ).astype(jnp.bfloat16),
        SP,
        0,
    )
    following = jnp.concatenate([decay[1:], jnp.ones_like(decay[:1])], axis=0)
    through, local_grad = lax.associative_scan(
        chain_link, (following[::-1], state_grad[::-1]), axis=0
    )
    through = through[::-1]
    local_grad = local_grad[::-1]
    chain_mult = decay[0] * through[0]
    chain_add = decay[0] * local_grad[0]
    _, incoming = entering(
        (chain_mult, chain_add), SP, compose, (jnp.ones_like(chain_mult), jnp.zeros_like(chain_add))
    )
    carried = local_grad + through * incoming[None, :]
    rec_value_grad = (carried * scale_in * input_gate).astype(jnp.bfloat16)
    input_pre_grad = (carried * scale_in * signal * input_gate * (1.0 - input_gate)).astype(
        jnp.bfloat16
    )
    decay_part = decay * before_state - input_gate * signal * decay * decay / scale_in
    rate_pre_grad = (
        carried * decay_part * (-decay_scale * decay_speed) * rate_gate * (1.0 - rate_gate)
    ).astype(jnp.bfloat16)
    return (
        expert_out[0][None],
        expert_out[1][None],
        expert_out[2][None],
        out_proj_grad,
        rec_value_grad,
        rate_pre_grad,
        input_pre_grad,
    )


def solution(mesh):
    finer = Mesh(mesh.devices.reshape(8, 4, mesh.shape["tp"]), ("sp_0", "sp_1", "tp"))
    placed = (
        P(SP, "tp"),
        P(SP, "tp"),
        P(SP, None),
        P(SP, None),
        P(SP, None, "tp"),
        P(SP, None, "tp"),
        P(SP, "tp", None),
        P("tp", None),
        P(SP, "tp"),
        P(SP, "tp"),
        P(SP, "tp"),
        P(SP, "tp"),
        P("tp"),
    )
    return jax.shard_map(
        per_device,
        mesh=finer,
        in_specs=placed,
        out_specs=(
            P(SP, None, "tp"),
            P(SP, None, "tp"),
            P(SP, "tp", None),
            P(SP, "tp"),
            P(SP, "tp"),
            P(SP, "tp"),
            P(SP, "tp"),
        ),
        check_vma=False,
    )
```

profile of v0, /device:TPU:1, one launch (start us, length us, event | category | flops | bytes accessed | tf_op | source)
XLA Modules:
  0.0 209.6 jit_solution(11607616895338328449)
XLA Ops:
  7.2 0.7 broadcast_multiply_fusion
  8.0 0.8 copy.33
  9.3 0.6 reduce-window.6
  10.2 1.4 scatter_custom_fusion.1
  11.7 1.4 scatter_custom_fusion
  13.1 1.9 gather_fusion.2
  15.0 1.9 gather_fusion.3
  16.9 0.8 copy.36
  17.8 2.5 %gather_fusion = f32[320]{0:T(512)S(1)} fusion(f32[256]{0:T(256)S(1)} %reshape.413, s32[1024]{0:T(1024)S(1)} %pad_clamp_fusion.1), kind=kCustom, calls=%fused_computation.2 | custom fusion | bytes 3840 | tf_op jit(solution)/shard_map/gather | solution.py:113
  20.6 24.8 %all_to_all.34 = bf16[32,10,256]{2,1,0:T(8,128)(2,1)S(1)} all-to-all(bf16[32,10,256]{2,1,0:T(8,128)(2,1)S(1)} %all_to_all.22), channel_id=1, replica_groups=mesh['sp_0'=8,'sp_1'=4,'tp'=16] {'sp_0','sp_1'}, dimensions={0} | all-to-all | bytes 327680 | tf_op jit(solution)/shard_map/all_to_all | solution.py:16
  45.5 0.7 pad_maximum_fusion.1
  46.2 43.0 %all-gather.6.cloned.1.call-done = bf16[640,2048]{1,0:T(8,128)(2,1)} async-done(((bf16[640,128]{1,0:T(8,128)(2,1)}), bf16[640,2048]{1,0:T(8,128)(2,1)}) %all-gather.6.cloned.1.call-update) | async-done | bytes 2621456 | tf_op jit(solution)/shard_map/all_gather | solution.py:32
  89.2 2.0 fusion.10
  91.2 1.8 fusion.12
  94.1 0.5 fusion.4
  94.6 1.4 copy.44
  96.0 5.0 %all-to-all-start.1 = ((bf16[16,320,128]{2,1,0:T(8,128)(2,1)}), bf16[16,320,128]{2,1,0:T(8,128)(2,1)S(1)}, u32[]{:S(2)}, u32[]{:S(2)}) async-start(bf16[16,320,128]{2,1,0:T(8,128)(2,1)} %bitcast.161), calls=%async_computation.1 | async-start | bytes 2621440 | tf_op jit(solution)/shard_map/all_to_all | solution.py:43
  101.7 2.7 %fusion.1 = bf16[1,2048,128]{2,1,0:T(8,128)(2,1)} fusion(bf16[320,128]{1,0:T(8,128)(2,1)S(1)} %get-tuple-element.11, bf16[640,2048]{1,0:T(8,128)(2,1)} %all-gather.6.cloned.1.call-done), kind=kOutput, calls=%fused_computation.12 | convolution fusion | flops 168034304 | bytes 1916928 | tf_op jit(solution)/shard_map/dot_general | solution.py:137
  104.4 2.6 %fusion.3 = bf16[1,128,2048]{2,1,0:T(8,128)(2,1)} fusion(bf16[640,2048]{1,0:T(8,128)(2,1)} %all-gather.6.cloned.1.call-done, f32[320,128]{1,0:T(8,128)S(1)} %fusion.12, f32[320,128]{1,0:T(8,128)S(1)} %fusion.10), kind=kOutput, calls=%fused_computation.14 | convolution fusion | flops 168280064 | bytes 2162688 | tf_op jit(solution)/shard_map/dot_general | solution.py:129
  107.1 27.2 %all-to-all-done.1 = bf16[16,320,128]{2,1,0:T(8,128)(2,1)S(1)} async-done(((bf16[16,320,128]{2,1,0:T(8,128)(2,1)}), bf16[16,320,128]{2,1,0:T(8,128)(2,1)S(1)}, u32[]{:S(2)}, u32[]{:S(2)}) %all-to-all-start.1) | async-done | bytes 1310752 | tf_op jit(solution)/shard_map/all_to_all | solution.py:43
  134.5 0.7 all_to_all.26
  135.2 9.9 %all-to-all-start.2 = ((bf16[32,10,128]{2,1,0:T(8,128)(2,1)}), bf16[32,10,128]{2,1,0:T(8,128)(2,1)S(1)}, u32[]{:S(2)}, u32[]{:S(2)}) async-start(bf16[32,10,128]{2,1,0:T(8,128)(2,1)} %all_to_all.26), calls=%async_computation.2 | async-start | bytes 262144 | tf_op jit(solution)/shard_map/all_to_all | solution.py:181
  145.1 2.8 %fusion.2 = bf16[1,2048,128]{2,1,0:T(8,128)(2,1)} fusion(bf16[320,128]{1,0:T(8,128)(2,1)S(1)} %get-tuple-element.10, bf16[640,2048]{1,0:T(8,128)(2,1)} %all-gather.6.cloned.1.call-done), kind=kOutput, calls=%fused_computation.13 | convolution fusion | flops 168034304 | bytes 1916928 | tf_op jit(solution)/shard_map/dot_general | solution.py:140
  147.9 7.7 %all-to-all-done.2 = bf16[32,10,128]{2,1,0:T(8,128)(2,1)S(1)} async-done(((bf16[32,10,128]{2,1,0:T(8,128)(2,1)}), bf16[32,10,128]{2,1,0:T(8,128)(2,1)S(1)}, u32[]{:S(2)}, u32[]{:S(2)}) %all-to-all-start.2) | async-done | bytes 81952 | tf_op jit(solution)/shard_map/all_to_all | solution.py:181
  155.6 0.9 gather_fusion.1
  156.7 16.2 %all_gather.19 = bf16[128,2048]{1,0:T(8,128)(2,1)S(1)} all-gather(bf16[128,128]{1,0:T(8,128)(2,1)S(1)} %add_convert_fusion), channel_id=1, replica_groups=mesh['sp_0'=8,'sp_1'=4,'tp'=16] {'tp'}, dimensions={1}, use_global_device_ids=true | all-gather | bytes 557056 | tf_op jit(solution)/shard_map/all_gather | solution.py:183
  174.1 1.2 convolution_convert_fusion
  175.3 3.9 %all-to-all-start.3 = ((bf16[32,64,128]{2,1,0:T(8,128)(2,1)}), bf16[32,64,128]{2,1,0:T(8,128)(2,1)S(1)}, u32[]{:S(2)}, u32[]{:S(2)}) async-start(bf16[32,64,128]{2,1,0:T(8,128)(2,1)} %bitcast.11), calls=%async_computation.3 | async-start | bytes 1048576 | tf_op jit(solution)/shard_map/all_to_all | solution.py:43
  180.0 8.3 %all-gather.2 = f32[4,2,128]{2,1,0:T(2,128)S(1)} all-gather(f32[1,2,128]{2,1,0:T(2,128)S(1)} %maximum_bitcast_fusion), channel_id=2, replica_groups=mesh['sp_0'=8,'sp_1'=4,'tp'=16] {'sp_1'}, dimensions={0}, use_global_device_ids=true | all-gather | bytes 5120 | tf_op jit(solution)/shard_map/all_gather | solution.py:61
  188.3 13.0 %all-gather.3 = f32[8,2,128]{2,1,0:T(2,128)S(1)} all-gather(f32[1,2,128]{2,1,0:T(2,128)S(1)} %maximum_bitcast_fusion.1), channel_id=3, replica_groups=mesh['sp_0'=8,'sp_1'=4,'tp'=16] {'sp_0'}, dimensions={0}, use_global_device_ids=true | all-gather | bytes 9216 | tf_op jit(solution)/shard_map/all_gather | solution.py:61
  201.3 0.8 fusion.26
  202.1 0.7 convert_reduce_fusion
  (184 shorter events, 5.0 us)
Async XLA Ops:
  7.2 82.1 %copy-start = (bf16[1,2048,128]{2,1,0:T(8,128)(2,1)S(1)}, bf16[1,2048,128]{2,1,0:T(8,128)(2,1)}, u32[]{:S(2)}) copy-start(bf16[1,2048,128]{2,1,0:T(8,128)(2,1)} %param.19) | copy-start | bytes 1572868
  7.2 82.0 %all-gather.6.cloned.1.call-start = ((), (), s32[]{:S(2)}) async-start(), calls=%async_computation.4 | async-start | bytes 2785280 | tf_op jit(solution)/shard_map/all_gather | solution.py:32
  20.3 70.9 %copy-start.3 = (bf16[1,2048,128]{2,1,0:T(8,128)(2,1)S(1)}, bf16[1,2048,128]{2,1,0:T(8,128)(2,1)}, u32[]{:S(2)}) copy-start(bf16[1,2048,128]{2,1,0:T(8,128)(2,1)} %param.20) | copy-start | bytes 1572868
  45.5 47.5 %copy-start.10 = (bf16[1,128,2048]{2,1,0:T(8,128)(2,1)S(1)}, bf16[1,128,2048]{2,1,0:T(8,128)(2,1)}, u32[]{:S(2)}) copy-start(bf16[1,128,2048]{2,1,0:T(8,128)(2,1)} %param.21) | copy-start | bytes 1572868
  89.2 3.8 %copy-start.2 = (bf16[640,2048]{1,0:T(8,128)(2,1)S(1)}, bf16[640,2048]{1,0:T(8,128)(2,1)}, u32[]{:S(2)}) copy-start(bf16[640,2048]{1,0:T(8,128)(2,1)} %all-gather.6.cloned.1.call-done) | copy-start | bytes 7864324
  94.6 6.6 %copy-start.11 = (f32[128]{0:T(128)S(1)}, f32[128]{0:T(128)}, u32[]{:S(2)}) copy-start(f32[128]{0:T(128)} %param.27) | copy-start | bytes 1540
  94.6 6.6 %copy-start.5 = (bf16[128,128]{1,0:T(8,128)(2,1)S(1)}, bf16[128,128]{1,0:T(8,128)(2,1)}, u32[]{:S(2)}) copy-start(bf16[128,128]{1,0:T(8,128)(2,1)} %param.24) | copy-start | bytes 98308
  94.6 6.8 %copy-start.9 = (s32[128,2]{0,1:T(2,128)S(1)}, s32[128,2]{0,1:T(2,128)}, u32[]{:S(2)}) copy-start(s32[128,2]{0,1:T(2,128)} %param.17) | copy-start | bytes 3076
  96.0 38.2 %all-to-all-start.1 = ((bf16[16,320,128]{2,1,0:T(8,128)(2,1)}), bf16[16,320,128]{2,1,0:T(8,128)(2,1)S(1)}, u32[]{:S(2)}, u32[]{:S(2)}) async-start(bf16[16,320,128]{2,1,0:T(8,128)(2,1)} %bitcast.161), calls=%async_computation.1 | async-start | bytes 2621440 | tf_op jit(solution)/shard_map/all_to_all | solution.py:43
  107.1 49.7 %copy-start.1 = (bf16[128,128]{1,0:T(8,128)(2,1)S(1)}, bf16[128,128]{1,0:T(8,128)(2,1)}, u32[]{:S(2)}) copy-start(bf16[128,128]{1,0:T(8,128)(2,1)} %param.16) | copy-start | bytes 98308
  107.1 65.9 %copy-start.4 = (bf16[128,2048]{1,0:T(8,128)(2,1)S(1)}, bf16[128,2048]{1,0:T(8,128)(2,1)}, u32[]{:S(2)}) copy-start(bf16[128,2048]{1,0:T(8,128)(2,1)} %param.22) | copy-start | bytes 1572868
  135.2 20.4 %all-to-all-start.2 = ((bf16[32,10,128]{2,1,0:T(8,128)(2,1)}), bf16[32,10,128]{2,1,0:T(8,128)(2,1)S(1)}, u32[]{:S(2)}, u32[]{:S(2)}) async-start(bf16[32,10,128]{2,1,0:T(8,128)(2,1)} %all_to_all.26), calls=%async_computation.2 | async-start | bytes 262144 | tf_op jit(solution)/shard_map/all_to_all | solution.py:181
  145.1 29.0 %copy-start.6 = (bf16[128,128]{1,0:T(8,128)(2,1)S(1)}, bf16[128,128]{1,0:T(8,128)(2,1)}, u32[]{:S(2)}) copy-start(bf16[128,128]{1,0:T(8,128)(2,1)} %param.23) | copy-start | bytes 98308
  145.1 29.0 %copy-start.7 = (bf16[128,128]{1,0:T(8,128)(2,1)S(1)}, bf16[128,128]{1,0:T(8,128)(2,1)}, u32[]{:S(2)}) copy-start(bf16[128,128]{1,0:T(8,128)(2,1)} %param.26) | copy-start | bytes 98308
  145.1 29.0 %copy-start.8 = (bf16[128,128]{1,0:T(8,128)(2,1)S(1)}, bf16[128,128]{1,0:T(8,128)(2,1)}, u32[]{:S(2)}) copy-start(bf16[128,128]{1,0:T(8,128)(2,1)} %param.25) | copy-start | bytes 98308
  175.3 26.8 %all-to-all-start.3 = ((bf16[32,64,128]{2,1,0:T(8,128)(2,1)}), bf16[32,64,128]{2,1,0:T(8,128)(2,1)S(1)}, u32[]{:S(2)}, u32[]{:S(2)}) async-start(bf16[32,64,128]{2,1,0:T(8,128)(2,1)} %bitcast.11), calls=%async_computation.3 | async-start | bytes 1048576 | tf_op jit(solution)/shard_map/all_to_all | solution.py:43
Sparse Core Ops, SparseCore 0:
  46.4 42.8 all-gather.5
where the time goes:
time: 213 us; the launch traced here: 210 us
  waiting for transfers between devices  77.9 us (37%)
  blocking collectives  62.3 us (29%)
  starting transfers between devices  18.8 us (9%)
  local copies, waits for them, and re-layouts  15.8 us (7%)
  between operations  15.1 us (7%)
  matrix products  14.9 us (7%)
  other arithmetic  4.78 us (2%)
    all_gather x1, waiting for transfers between devices, sent_together(): lax.all_gather(both, axis, axis=dim, tiled=True)  43 us
    all_to_all x2, waiting for transfers between devices, sent_and_summed(): lax.all_to_all(tiles, axis, split_axis=0, concat_axis=0, tiled=True)  27.2 us
    all_to_all x1, blocking collectives, in_one_piece(): lax.all_to_all(both, axis, split_axis=split_dim, concat_axis=concat_dim,...  24.8 us
    all_gather x2, blocking collectives, all_in_one(): both, at, found = (lax.all_gather(jnp.concatenate(lines), axis), 0, {})  21.2 us
    all_gather x1, blocking collectives, per_device(): mix_grad = lax.all_gather(own_grad, 'tp', axis=1, tiled=True)  16.2 us
    all_to_all x1, starting transfers between devices, per_device(): lax.all_to_all(summed_share, SP, split_axis=0, concat_axis=0, tiled=True)  9.9 us
    all_to_all x2, starting transfers between devices, sent_and_summed(): lax.all_to_all(tiles, axis, split_axis=0, concat_axis=0, tiled=True)  8.87 us
    all_to_all x1, waiting for transfers between devices, per_device(): lax.all_to_all(summed_share, SP, split_axis=0, concat_axis=0, tiled=True)  7.7 us
  transfers between devices with their start and end apart: 4, of which 3 were waited for; matrix products, arithmetic and copies ran while one was open for 5% of the time, Pallas kernels for 0%

commit v1 on v0

v1 whole, which is shorter than its diff:
```python
import functools

import jax
import jax.numpy as jnp
from jax import lax
from jax.experimental import pallas as pl
from jax.experimental.pallas import tpu as pltpu
from jax.sharding import PartitionSpec as P

MESH = pl.DeviceIdType.MESH
F32 = jnp.float32
BF = jnp.bfloat16
decay_scale = 8.0
SLOT_PAD = 16
LANES = 128


def dot(a, b, ca, cb):
    return lax.dot_general(a, b, (((ca,), (cb,)), ((), ())), preferred_element_type=F32)


def expm1_neg(v):
    near = jnp.ones_like(v)
    for n in range(9, 1, -1):
        near = 1.0 + v * near * (1.0 / n)
    return jnp.where(v > -0.5, v * near, jnp.exp(v) - 1.0)


def step_kernel(
    dims,
    x_ref,
    cot_ref,
    rt_ref,
    rw_ref,
    gw_hbm,
    uw_hbm,
    dw_hbm,
    op_hbm,
    rv_ref,
    rp_ref,
    ip_ref,
    ps_ref,
    dp_ref,
    gwg_hbm,
    uwg_hbm,
    dwg_hbm,
    opg_ref,
    rvg_ref,
    rpg_ref,
    ipg_ref,
    wgu,
    wpart,
    dw,
    op,
    onehot,
    send1,
    recv1,
    inf,
    cotf,
    acc,
    hacc,
    grads,
    grads_p,
    hid,
    part,
    rss,
    rsr,
    send5,
    recv5,
    mixf,
    sg,
    levels,
    through,
    coef,
    rec,
    xsend,
    xrecv,
    zsend,
    zrecv,
    chs,
    chr_,
    ogu,
    odw,
    w_sem,
    o_sem,
    wp_s,
    wp_r,
    p1_s,
    p1_r,
    y_s,
    y_r,
    d_s,
    d_r,
    g_s,
    g_r,
    q_s,
    q_r,
    p5_s,
    p5_r,
    m_s,
    m_r,
    md_s,
    md_r,
    x_s,
    x_r,
    z_s,
    z_r,
    c_s,
    c_r,
):
    SPN, NX, NY, E, CAP, TD, R = dims
    NZ = SPN // NX
    RH = R // 2
    EH = E // 2
    CP = SLOT_PAD
    H = NY // 2
    s = lax.axis_index("sp")
    t = lax.axis_index("tp")
    y = t // 2
    c = t % 2
    z = s // NX
    x = s % NX

    def remote(src, dst, ss, rs, dev):
        return pltpu.make_async_remote_copy(
            src_ref=src, dst_ref=dst, send_sem=ss, recv_sem=rs, device_id=dev, device_id_type=MESH
        )

    def at_y(j):
        return (s, lax.rem(y + j + NY, NY) * 2 + c)

    partner = (s, y * 2 + 1 - c)

    def at_sp(j):
        return (lax.rem(s + j + SPN, SPN), t)

    def took(ref, sem):
        pltpu.make_async_copy(ref, ref, sem).wait()

    barrier = pltpu.get_barrier_semaphore()

    def greet(k, carry):
        pl.semaphore_signal(barrier, inc=1, device_id=at_sp(k), device_id_type=MESH)
        return carry

    lax.fori_loop(1, SPN, greet, 0)
    for j in range(1, NY):
        pl.semaphore_signal(barrier, inc=1, device_id=at_y(j), device_id_type=MESH)
    pl.semaphore_signal(barrier, inc=1, device_id=partner, device_id_type=MESH)

    loads = [
        pltpu.make_async_copy(gw_hbm, wgu.at[:, pl.ds(0, LANES)], w_sem.at[0]),
        pltpu.make_async_copy(uw_hbm, wgu.at[:, pl.ds(LANES, LANES)], w_sem.at[1]),
        pltpu.make_async_copy(dw_hbm, dw, w_sem.at[2]),
        pltpu.make_async_copy(op_hbm, op, w_sem.at[3]),
    ]
    for load in loads:
        load.start()

    rows = lax.broadcasted_iota(jnp.int32, (TD, TD), 0)
    cols = lax.broadcasted_iota(jnp.int32, (TD, TD), 1)
    earlier = (rows > cols).astype(BF)
    lane = lax.broadcasted_iota(jnp.int32, (TD, LANES), 1)
    r0, r1 = rt_ref[:, 0:1], rt_ref[:, 1:2]
    marks0 = (lane == r0).astype(F32)
    marks1 = (lane == r1).astype(F32)
    before = dot(earlier, (marks0 + marks1).astype(BF), 1, 0)
    slots = lax.broadcasted_iota(jnp.int32, (TD, E * CP), 1)

    def picks(r, marks):
        rank = jnp.sum(before * marks, axis=1, keepdims=True).astype(jnp.int32)
        away = jnp.where(r <= s, s - r, s - r + SPN)
        return (slots == away * CP + rank).astype(F32)

    pick0 = picks(r0, marks0)
    pick1 = picks(r1, marks1)
    both = (pick0 + pick1).astype(BF)
    onehot[...] = both
    cot = cot_ref[...].astype(F32)
    sc0 = (rw_ref[:, 0:1] * cot).astype(BF)
    sc1 = (rw_ref[:, 1:2] * cot).astype(BF)
    row_in = dot(both, x_ref[...], 0, 0).astype(BF)
    row_cot = (dot(pick0.astype(BF), sc0, 0, 0) + dot(pick1.astype(BF), sc1, 0, 0)).astype(BF)
    send1[:, :, 0:LANES] = row_in.reshape(E, CP, LANES)
    send1[:, :, LANES:] = row_cot.reshape(E, CP, LANES)
    recv1[0] = send1[0]

    pl.semaphore_wait(barrier, SPN - 1 + NY - 1 + 1)

    def all_sent(src_of, dst_of, ss, rs, sign):
        def go(k):
            remote(src_of(k), dst_of(k), ss, rs, at_sp(sign * k)).start()

        def pair(k, carry):
            go(k)
            go(SPN - k)
            return carry

        lax.fori_loop(1, SPN // 2, pair, 0)
        go(SPN // 2)

    all_sent(lambda k: send1.at[k], lambda k: recv1.at[k], p1_s, p1_r, -1)

    loads[0].wait()
    loads[1].wait()
    for j in range(NY):
        remote(
            wgu.at[pl.ds(pl.multiple_of(j * 256 + (1 - c) * LANES, LANES), LANES), :],
            wpart.at[j],
            wp_s,
            wp_r,
            partner,
        ).start()
    loads[2].wait()
    loads[3].wait()

    decay_speed = jnp.log1p(jnp.exp(-dp_ref[...]))
    rate = jax.nn.sigmoid(rp_ref[...].astype(F32))
    inlet = jax.nn.sigmoid(ip_ref[...].astype(F32))
    signal = rv_ref[...].astype(F32)
    prev = ps_ref[...].astype(F32)
    log_decay = -decay_scale * rate * decay_speed
    decay = jnp.exp(log_decay)
    scale_in = jnp.sqrt(-expm1_neg(2.0 * log_decay))
    rec[...] = (decay * prev + scale_in * inlet * signal).astype(BF)
    gain = scale_in * inlet
    coef[0] = gain
    coef[1] = gain * signal * (1.0 - inlet)
    slope = decay * prev - inlet * signal * decay * decay / scale_in
    coef[2] = slope * (-decay_scale * decay_speed) * rate * (1.0 - rate)
    tok = lax.broadcasted_iota(jnp.int32, (TD, LANES), 0)
    span = jnp.where(tok < TD - 1, pltpu.roll(decay, TD - 1, 0), 1.0)
    n_levels = TD.bit_length() - 1
    for k in range(n_levels):
        inside = tok < TD - (1 << k)
        levels[k] = jnp.where(inside, span, 0.0)
        span = span * jnp.where(inside, pltpu.roll(span, TD - (1 << k), 0), 1.0)
    through[...] = span
    first_decay = decay[0:1, :]
    chs[0:1, :] = first_decay * span[0:1, :]

    half_i = lax.broadcasted_iota(jnp.int32, (RH, EH * CP), 0)
    half_j = lax.broadcasted_iota(jnp.int32, (RH, EH * CP), 1)
    slot_of = half_j & (CP - 1)
    dense = jnp.where(slot_of < CAP, (half_j >> 4) * CAP + slot_of, -1)
    sel = (half_i == dense).astype(BF)

    took(recv1.at[pl.ds(1, SPN - 1)], p1_r)
    for h in range(2):
        got = recv1[pl.ds(h * EH, EH)].reshape(EH * CP, 2 * LANES)
        kept = dot(sel, got, 1, 0).astype(BF)
        inf[0, c, pl.ds(h * RH, RH), :] = kept[:, :LANES]
        cotf[0, c, pl.ds(h * RH, RH), :] = kept[:, LANES:]

    bufs = (inf, cotf)
    DIR = (1, -1)

    def hops(di, piece):
        return H if di == piece else H - 1

    def ring(piece, di, h):
        src = (-DIR[di] * h) % NY
        dst = (-DIR[di] * (h + 1)) % NY
        buf = bufs[piece]
        return remote(
            buf.at[src, c], buf.at[dst, c], y_s.at[di, piece, h], y_r.at[di, piece, h], at_y(DIR[di])
        )

    def across(piece, slot):
        buf = bufs[piece]
        return remote(
            buf.at[slot, c], buf.at[slot, c], d_s.at[piece, slot], d_r.at[piece, slot], partner
        )

    for piece in range(2):
        for di in range(2):
            if hops(di, piece):
                ring(piece, di, 0).start()
        across(piece, 0).start()

    acc[...] = jnp.zeros_like(acc)
    hacc[...] = jnp.zeros_like(hacc)

    def y_at(j):
        return lax.rem(y + j, NY)

    def rows_at(j, wide):
        return pl.ds(pl.multiple_of(y_at(j) * wide, wide), wide)

    def forward_chunk(j):
        across(0, j).wait_recv()
        rows_in = jnp.concatenate([inf[j, 0], inf[j, 1]], axis=1)
        acc[...] += dot(rows_in, wgu[rows_at(j, 256), :], 1, 0)
        across(1, j).wait_recv()
        rows_cot = jnp.concatenate([cotf[j, 0], cotf[j, 1]], axis=1)
        hacc[...] += dot(rows_cot, dw[:, rows_at(j, 256)], 1, 1)

    def at_distance(d):
        return sorted({d % NY, -d % NY})

    for h in range(H):
        for piece in range(2):
            for di in range(2):
                if h < hops(di, piece):
                    ring(piece, di, h).wait_recv()
                    if h + 1 < hops(di, piece):
                        ring(piece, di, h + 1).start()
                    across(piece, (-DIR[di] * (h + 1)) % NY).start()
        for j in at_distance(h):
            forward_chunk(j)
    forward_chunk(H)

    for h in range(2):
        at = pl.ds(h * RH, RH)
        gate_act = acc[at, :LANES]
        up_act = acc[at, LANES:]
        hidden_grad = hacc[at, :]
        squash = jax.nn.sigmoid(gate_act)
        silu_gate = gate_act * squash
        hid[at, :] = (silu_gate * up_act).astype(BF)
        grads[at, :LANES] = (
            hidden_grad * up_act * squash * (1.0 + gate_act * (1.0 - squash))
        ).astype(BF)
        grads[at, LANES:] = (hidden_grad * silu_gate).astype(BF)
    swap = remote(grads, grads_p, g_s, g_r, partner)
    swap.start()

    waited = []

    def term(j):
        own = wgu[pl.ds(pl.multiple_of(y_at(j) * 256 + c * LANES, LANES), LANES), :]
        value = dot(grads[...], own, 1, 1)
        if not waited:
            swap.wait_recv()
            took(wpart, wp_r)
            waited.append(1)
        part[j] = value + dot(grads_p[...], wpart[y_at(j)], 1, 1)

    def weight_grads(j):
        rows_in = jnp.concatenate([inf[j, 0], inf[j, 1]], axis=1)
        ogu[rows_at(j, 256), :] = dot(rows_in, grads[...], 0, 0).astype(BF)
        rows_cot = jnp.concatenate([cotf[j, 0], cotf[j, 1]], axis=1)
        odw[:, rows_at(j, 256)] = dot(hid[...], rows_cot, 0, 0).astype(BF)

    def chain(di, half, k):
        return remote(
            rss.at[di, half, k],
            rsr.at[di, half, k],
            q_s.at[di, half, k],
            q_r.at[di, half, k],
            at_y(DIR[di]),
        )

    ready = set()

    def need(j):
        if j not in ready:
            ready.add(j)
            term(j)

    left = list(range(NY))
    for k in range(H + 1):
        for half, di in ((0, 0), (1, 1), (1, 0), (0, 1)):
            n = hops(di, half)
            if k < n:
                j = (DIR[di] * (n - k)) % NY
                need(j)
                value = part[j, pl.ds(half * RH, RH), :]
                if k:
                    chain(di, half, k - 1).wait_recv()
                    value = value + rsr[di, half, k - 1].astype(F32)
                rss[di, half, k] = value.astype(BF)
                chain(di, half, k).start()
        if k < H:
            for half, di in ((0, 0), (1, 1), (1, 0), (0, 1)):
                n = hops(di, half)
                if k + 1 < n:
                    need((DIR[di] * (n - k - 1)) % NY)
            for j in left[: -(-NY // H)]:
                weight_grads(j)
            left = left[-(-NY // H) :]
    need(0)
    outs = [
        pltpu.make_async_copy(ogu.at[:, pl.ds(0, LANES)], gwg_hbm, o_sem.at[0]),
        pltpu.make_async_copy(ogu.at[:, pl.ds(LANES, LANES)], uwg_hbm, o_sem.at[1]),
        pltpu.make_async_copy(odw, dwg_hbm, o_sem.at[2]),
    ]
    for half in range(2):
        value = part[0, pl.ds(half * RH, RH), :]
        for di in range(2):
            n = hops(di, half)
            if n:
                chain(di, half, n - 1).wait_recv()
                value = value + rsr[di, half, n - 1].astype(F32)
        spread = dot(sel, value.astype(BF), 0, 0).astype(BF)
        send5[pl.ds(half * EH, EH)] = spread.reshape(EH, CP, LANES)
    recv5[0] = send5[0]
    all_sent(lambda k: send5.at[k], lambda k: recv5.at[k], p5_s, p5_r, 1)
    for out in outs:
        out.start()
    took(recv5.at[pl.ds(1, SPN - 1)], p5_r)
    returned = dot(onehot[...], recv5[...].reshape(E * CP, LANES), 1, 0)
    mixf[0, c] = (returned + cot_ref[...].astype(F32)).astype(BF)

    def mix_to(j):
        dst = (-j) % NY
        return remote(mixf.at[0, c], mixf.at[dst, c], m_s.at[dst], m_r.at[dst], at_y(j))

    def mix_across(slot):
        return remote(mixf.at[slot, c], mixf.at[slot, c], md_s.at[slot], md_r.at[slot], partner)

    order = [0]
    for d in range(1, H + 1):
        order += at_distance(d)
    for j in order[:0:-1]:
        mix_to(j).start()
    mix_across(0).start()
    sg[...] = jnp.zeros_like(sg)

    def mixer_chunk(j):
        mix_across(j).wait_recv()
        rows_mix = jnp.concatenate([mixf[j, 0], mixf[j, 1]], axis=1)
        outer = dot(rows_mix, rec[...], 0, 0).astype(BF)
        xsend[j] = outer.reshape(NX, 256 // NX, LANES)
        for dx in range(1, NX):
            to = lax.rem(x + dx, NX)
            remote(
                xsend.at[j, to], xrecv.at[dx, j], x_s, x_r, (z * NX + to, t)
            ).start()
        sg[...] += dot(rows_mix, op[:, rows_at(j, 256)], 1, 1)

    behind = None
    for j in order:
        if j:
            mix_to((-j) % NY).wait_recv()
            mix_across(j).start()
        if behind is not None:
            mixer_chunk(behind)
        behind = j
    mixer_chunk(behind)

    local = sg[...]
    for k in range(n_levels):
        local = local + levels[k] * pltpu.roll(local, TD - (1 << k), 0)
    chs[1:2, :] = first_decay * local[0:1, :]
    all_sent(lambda k: chs, lambda k: chr_.at[k], c_s, c_r, -1)

    took(xrecv.at[pl.ds(1, NX - 1)], x_r)
    mine = None
    for dz in range(NZ):
        to_z = lax.rem(z + dz, NZ)
        j = lax.rem(to_z - y + NY, NY)
        total = xsend[j, x].astype(F32)
        for dx in range(1, NX):
            total = total + xrecv[dx, j].astype(F32)
        if dz == 0:
            mine = total
        else:
            zsend[dz] = total.astype(BF)
            remote(zsend.at[dz], zrecv.at[dz], z_s, z_r, (to_z * NX + x, t)).start()

    took(chr_.at[pl.ds(1, SPN - 1)], c_r)
    entering = jnp.zeros((1, LANES), F32)
    for k in range(SPN - 1, 0, -1):
        entering = jnp.where(s + k < SPN, chr_[k, 1:2, :] + chr_[k, 0:1, :] * entering, entering)
    carried = local + through[...] * entering
    rvg_ref[...] = (carried * coef[0]).astype(BF)
    ipg_ref[...] = (carried * coef[1]).astype(BF)
    rpg_ref[...] = (carried * coef[2]).astype(BF)

    took(zrecv.at[pl.ds(1, NZ - 1)], z_r)
    for dz in range(1, NZ):
        mine = mine + zrecv[dz].astype(F32)
    opg_ref[...] = mine

    took(recv1.at[pl.ds(1, SPN - 1)], p1_s)
    took(wpart, wp_s)
    for piece in range(2):
        for di in range(2):
            for h in range(hops(di, piece)):
                ring(piece, di, h).wait_send()
                chain(di, piece, h).wait_send()
        for j in range(NY):
            across(piece, j).wait_send()
    swap.wait_send()
    took(recv5.at[pl.ds(1, SPN - 1)], p5_s)
    for j in range(1, NY):
        mix_to(j).wait_send()
    for j in range(NY):
        mix_across(j).wait_send()
    took(xrecv.at[pl.ds(1, NX - 1)], x_s)
    took(zrecv.at[pl.ds(1, NZ - 1)], z_s)
    took(chr_.at[pl.ds(1, SPN - 1)], c_s)
    for out in outs:
        out.wait()


def solution(mesh):
    SPN, TPN = mesh.shape["sp"], mesh.shape["tp"]
    NX = 4 if SPN == 32 else 2
    NZ, NY = SPN // NX, TPN // 2

    def per_device(
        ffn_input,
        out_grad,
        routes,
        route_weight,
        gate_w,
        up_w,
        down_w,
        out_proj,
        rec_value,
        rate_pre,
        input_pre,
        prev_state,
        decay_param,
    ):
        TD, top = routes.shape
        E = SPN
        CAP = 5 * top * TD // (4 * E)
        R = E * CAP
        RH = R // 2
        D = gate_w.shape[1]
        H = NY // 2
        CP = SLOT_PAD
        vmem = pl.BlockSpec(memory_space=pltpu.VMEM)
        hbm = pl.BlockSpec(memory_space=pl.ANY)
        dma = pltpu.SemaphoreType.DMA
        levels = TD.bit_length() - 1
        scratch = [
            pltpu.VMEM((D, 256), BF),
            pltpu.VMEM((NY, LANES, 256), BF),
            pltpu.VMEM((LANES, D), BF),
            pltpu.VMEM((LANES, D), BF),
            pltpu.VMEM((TD, E * CP), BF),
            pltpu.VMEM((E, CP, 256), BF),
            pltpu.VMEM((E, CP, 256), BF),
            pltpu.VMEM((NY, 2, R, LANES), BF),
            pltpu.VMEM((NY, 2, R, LANES), BF),
            pltpu.VMEM((R, 256), F32),
            pltpu.VMEM((R, LANES), F32),
            pltpu.VMEM((R, 256), BF),
            pltpu.VMEM((R, 256), BF),
            pltpu.VMEM((R, LANES), BF),
            pltpu.VMEM((NY, R, LANES), F32),
            pltpu.VMEM((2, 2, H, RH, LANES), BF),
            pltpu.VMEM((2, 2, H, RH, LANES), BF),
            pltpu.VMEM((E, CP, LANES), BF),
            pltpu.VMEM((E, CP, LANES), BF),
            pltpu.VMEM((NY, 2, TD, LANES), BF),
            pltpu.VMEM((TD, LANES), F32),
            pltpu.VMEM((levels, TD, LANES), F32),
            pltpu.VMEM((TD, LANES), F32),
            pltpu.VMEM((3, TD, LANES), F32),
            pltpu.VMEM((TD, LANES), BF),
            pltpu.VMEM((NY, NX, 256 // NX, LANES), BF),
            pltpu.VMEM((NX, NY, 256 // NX, LANES), BF),
            pltpu.VMEM((NZ, 256 // NX, LANES), BF),
            pltpu.VMEM((NZ, 256 // NX, LANES), BF),
            pltpu.VMEM((2, LANES), F32),
            pltpu.VMEM((SPN, 2, LANES), F32),
            pltpu.VMEM((D, 256), BF),
            pltpu.VMEM((LANES, D), BF),
            dma((4,)),
            dma((3,)),
            dma,
            dma,
            dma,
            dma,
            dma((2, 2, H)),
            dma((2, 2, H)),
            dma((2, NY)),
            dma((2, NY)),
            dma,
            dma,
            dma((2, 2, H)),
            dma((2, 2, H)),
            dma,
            dma,
            dma((NY,)),
            dma((NY,)),
            dma((NY,)),
            dma((NY,)),
            dma,
            dma,
            dma,
            dma,
            dma,
            dma,
        ]
        shape = jax.ShapeDtypeStruct
        outs = pl.pallas_call(
            functools.partial(step_kernel, (SPN, NX, NY, E, CAP, TD, R)),
            out_shape=(
                shape((D, LANES), BF),
                shape((D, LANES), BF),
                shape((LANES, D), BF),
                shape((256 // NX, LANES), F32),
                shape((TD, LANES), BF),
                shape((TD, LANES), BF),
                shape((TD, LANES), BF),
            ),
            in_specs=[vmem] * 4 + [hbm] * 4 + [vmem] * 5,
            out_specs=[hbm] * 3 + [vmem] * 4,
            scratch_shapes=scratch,
            compiler_params=pltpu.CompilerParams(collective_id=0, has_side_effects=True),
        )(
            ffn_input,
            out_grad,
            routes,
            route_weight,
            gate_w[0],
            up_w[0],
            down_w[0],
            out_proj,
            rec_value,
            rate_pre,
            input_pre,
            prev_state,
            decay_param.reshape(1, -1),
        )
        return (outs[0][None], outs[1][None], outs[2][None], *outs[3:])

    tokens = P("sp", "tp")
    placed = (
        tokens,
        tokens,
        P("sp", None),
        P("sp", None),
        P("sp", None, "tp"),
        P("sp", None, "tp"),
        P("sp", "tp", None),
        P("tp", None),
        tokens,
        tokens,
        tokens,
        tokens,
        P("tp"),
    )
    return jax.shard_map(
        per_device,
        mesh=mesh,
        in_specs=placed,
        out_specs=(
            P("sp", None, "tp"),
            P("sp", None, "tp"),
            P("sp", "tp", None),
            tokens,
            tokens,
            tokens,
            tokens,
        ),
        check_vma=False,
    )
```

time: 213 us -> 99.6 us (0.47); the launches traced: 210 us -> 99.1 us
  Pallas kernels: 0 us -> 89.4 us
  waiting for transfers between devices: 77.9 us -> 0 us
  blocking collectives: 62.3 us -> 0 us
  starting transfers between devices: 18.8 us -> 0 us
  matrix products: 14.9 us -> 0 us
  between operations: 15.1 us -> 0.67 us
  local copies, waits for them, and re-layouts: 15.8 us -> 9.04 us
  other arithmetic: 4.78 us -> 0 us
    pallas_call x0 -> x1, Pallas kernels: none -> 89.4 us  [per_device(): pl.pallas_call(functools.partial(step_kernel, (SPN, NX, NY, E, CAP, TD, R...]
    all_gather x1 -> x0, waiting for transfers between devices: 43 us -> none  [sent_together(): lax.all_gather(both, axis, axis=dim, tiled=True)]
    all_gather x3 -> x0, blocking collectives: 37.5 us -> none  [the longest x2 21.2 us: all_in_one(): both, at, found = (lax.all_gather(jnp.concatenate(lines), axis), 0, {})]
    all_to_all x3 -> x0, waiting for transfers between devices: 34.9 us -> none  [the longest x2 27.2 us: sent_and_summed(): lax.all_to_all(tiles, axis, split_axis=0, concat_axis=0, tiled=True)]
    all_to_all x1 -> x0, blocking collectives: 24.8 us -> none  [in_one_piece(): lax.all_to_all(both, axis, split_axis=split_dim, concat_axis=concat_dim,...]
    all_to_all x3 -> x0, starting transfers between devices: 18.8 us -> none  [the longest x1 9.9 us: per_device(): lax.all_to_all(summed_share, SP, split_axis=0, concat_axis=0, tiled=True)]
    dot_general x10 -> x0, matrix products: 14.9 us -> none  [the longest x1 2.75 us: expert_work(): lax.dot_general(rows_in, up_grad, across, preferred_element_type=jnp.floa...]
    unnamed x26 -> x25, local copies, waits for them, and re-layouts: 1.64 us -> 9.04 us
  transfers between devices with their start and end apart: 4 -> 0, of which waited for: 3 -> 0; matrix products, arithmetic and copies ran while one was open for 5% -> 0% of each run, Pallas kernels for 0% -> 0%
where the time goes in v1:
time: 99.6 us; the launch traced here: 99.1 us
  Pallas kernels  89.4 us (90%)
  local copies, waits for them, and re-layouts  9.04 us (9%)
    pallas_call x1, Pallas kernels, per_device(): pl.pallas_call(functools.partial(step_kernel, (SPN, NX, NY, E, CAP, TD, R...  89.4 us
    unnamed x25, local copies, waits for them, and re-layouts  9.04 us

profile of v1, /device:TPU:1, one launch (start us, length us, event | category | flops | bytes accessed | tf_op | source)
XLA Modules:
  0.0 99.1 jit_solution(14331342042627980301)
XLA Ops:
  0.6 0.0 copy-start.6
  0.6 0.7 copy-done.6
  1.3 0.0 copy-start.7
  1.3 0.7 copy.20.rt_ref
  2.1 0.0 copy-done.7
  2.1 0.7 copy.21.rw_ref
  2.8 89.4 %shard_map.180 = (bf16[2048,128]{1,0:T(8,128)(2,1)}, bf16[2048,128]{1,0:T(8,128)(2,1)}, bf16[128,2048]{1,0:T(8,128)(2,1)}, f32[64,128]{1,0:T(8,128)}, bf16[128,1...) custom-call(bf16[128,128]{1,0:T(8,128)(2,1)} %x_ref.1, bf16[128,128]{1,0:T(8,128)(2,1)} %cot_ref.1, ...), custom_call_target="tpu_custom_call" | custom-call | tf_op jit(solution)/shard_map/pallas_call | solution.py:592
  92.2 0.0 copy-start.1
  92.2 1.9 %copy.29 = bf16[1,2048,128]{2,1,0:T(8,128)(2,1)} copy(bf16[1,2048,128]{2,1,0:T(8,128)(2,1)} %bitcast.9) | data formatting | bytes 1048576
  94.1 0.0 copy-done.1
  94.1 0.0 copy-start
  94.1 0.8 copy.30
  94.9 0.4 copy-done
  95.4 0.0 copy-start.5
  95.4 0.8 copy.31
  96.2 0.0 copy-done.5
  96.2 0.0 copy-start.4
  96.2 0.6 copy.32
  96.8 0.2 copy-done.4
  96.9 0.0 copy-start.3
  96.9 0.6 copy.33
  97.5 0.2 copy-done.3
  97.7 0.0 copy-start.2
  97.7 0.6 copy.34
  98.3 0.2 copy-done.2
  98.5 0.6 copy.35
Async XLA Ops:
  0.6 0.7 copy-start.6
  1.3 0.7 copy-start.7
  92.2 1.9 %copy-start.1 = (bf16[2048,128]{1,0:T(8,128)(2,1)S(1)}, bf16[2048,128]{1,0:T(8,128)(2,1)}, u32[]{:S(2)}) copy-start(bf16[2048,128]{1,0:T(8,128)(2,1)} %get-tuple-element.15) | copy-start | bytes 1572868
  94.1 1.2 %copy-start = (bf16[128,2048]{1,0:T(8,128)(2,1)S(1)}, bf16[128,2048]{1,0:T(8,128)(2,1)}, u32[]{:S(2)}) copy-start(bf16[128,2048]{1,0:T(8,128)(2,1)} %get-tuple-element.16) | copy-start | bytes 1572868
  95.4 0.8 copy-start.5
  96.2 0.8 copy-start.4
  96.9 0.8 copy-start.3
  97.7 0.8 copy-start.2

commit v2 on v1

v2 whole, which is shorter than its diff:
```python
import contextlib
import functools

import jax
import jax.numpy as jnp
from jax import lax
from jax.experimental import pallas as pl
from jax.experimental.pallas import tpu as pltpu
from jax.sharding import PartitionSpec as P


MESH = pl.DeviceIdType.MESH
F32 = jnp.float32
BF = jnp.bfloat16
decay_scale = 8.0
SCOPES = False
SLOT_PAD = 16
LANES = 128


def dot(a, b, ca, cb):
    return lax.dot_general(a, b, (((ca,), (cb,)), ((), ())), preferred_element_type=F32)


PHASE = contextlib.ExitStack()


def mark(name):
    if SCOPES:
        PHASE.close()
        if name:
            PHASE.enter_context(jax.named_scope(name))


def expm1_neg(v):
    near = jnp.ones_like(v)
    for n in range(9, 1, -1):
        near = 1.0 + v * near * (1.0 / n)
    return jnp.where(v > -0.5, v * near, jnp.exp(v) - 1.0)


def step_kernel(
    dims,
    x_hbm,
    cot_hbm,
    rt_hbm,
    rw_hbm,
    gw_hbm,
    uw_hbm,
    dw_hbm,
    op_hbm,
    rv_hbm,
    rp_hbm,
    ip_hbm,
    ps_hbm,
    dp_hbm,
    gwg_ref,
    uwg_ref,
    dwg_ref,
    opg_ref,
    rvg_ref,
    rpg_ref,
    ipg_ref,
    x_ref,
    cot_ref,
    rt_ref,
    rw_ref,
    rv_ref,
    rp_ref,
    ip_ref,
    ps_ref,
    dp_ref,
    wgu,
    wpart,
    dw,
    op,
    onehot,
    send1,
    recv1,
    inf,
    cotf,
    acc,
    hacc,
    grads,
    grads_p,
    hid,
    part,
    rss,
    rsr,
    send5,
    recv5,
    mixf,
    sg,
    levels,
    through,
    coef,
    rec,
    xsend,
    xrecv,
    zsum,
    zsend,
    zrecv,
    chs,
    chr_,
    w_sem,
    wp_s,
    wp_r,
    p1_s,
    p1_r,
    y_s,
    y_r,
    d_s,
    d_r,
    g_s,
    g_r,
    q_s,
    q_r,
    p5_s,
    p5_r,
    m_s,
    m_r,
    md_s,
    md_r,
    x_s,
    x_r,
    z_s,
    z_r,
    c_s,
    c_r,
):
    SPN, NX, NY, E, CAP, TD, R = dims
    NZ = SPN // NX
    RH = R // 2
    EH = E // 2
    CP = SLOT_PAD
    H = NY // 2
    s = lax.axis_index("sp")
    t = lax.axis_index("tp")
    y = t // 2
    c = t % 2
    z = s // NX
    x = s % NX

    def remote(src, dst, ss, rs, dev):
        return pltpu.make_async_remote_copy(
            src_ref=src, dst_ref=dst, send_sem=ss, recv_sem=rs, device_id=dev, device_id_type=MESH
        )

    def at_y(j):
        return (s, lax.rem(y + j + NY, NY) * 2 + c)

    partner = (s, y * 2 + 1 - c)

    def at_sp(j):
        return (lax.rem(s + j + SPN, SPN), t)

    def took(ref, sem):
        pltpu.make_async_copy(ref, ref, sem).wait()

    mark("start")
    loads = [
        pltpu.make_async_copy(src, dst, w_sem.at[n])
        for n, (src, dst) in enumerate(
            (
                (rt_hbm, rt_ref),
                (rw_hbm, rw_ref),
                (x_hbm, x_ref),
                (cot_hbm, cot_ref),
                (gw_hbm, wgu.at[:, pl.ds(0, LANES)]),
                (uw_hbm, wgu.at[:, pl.ds(LANES, LANES)]),
                (rv_hbm, rv_ref),
                (rp_hbm, rp_ref),
                (ip_hbm, ip_ref),
                (ps_hbm, ps_ref),
                (dp_hbm, dp_ref),
                (dw_hbm, dw),
                (op_hbm, op),
            )
        )
    ]
    for load in loads:
        load.start()

    barrier = pltpu.get_barrier_semaphore()

    def greet(k, carry):
        pl.semaphore_signal(barrier, inc=1, device_id=at_sp(k), device_id_type=MESH)
        return carry

    lax.fori_loop(1, SPN, greet, 0)
    for j in range(1, NY):
        pl.semaphore_signal(barrier, inc=1, device_id=at_y(j), device_id_type=MESH)
    pl.semaphore_signal(barrier, inc=1, device_id=partner, device_id_type=MESH)
    for load in loads[:4]:
        load.wait()

    mark("route")
    rows = lax.broadcasted_iota(jnp.int32, (TD, TD), 0)
    cols = lax.broadcasted_iota(jnp.int32, (TD, TD), 1)
    earlier = (rows < cols).astype(BF)
    ids = lax.broadcasted_iota(jnp.int32, (E, TD), 0)
    r0, r1 = rt_ref[0:1, :], rt_ref[1:2, :]
    marks0 = (ids == r0).astype(F32)
    marks1 = (ids == r1).astype(F32)
    before = dot((marks0 + marks1).astype(BF), earlier, 1, 0)
    slots = lax.broadcasted_iota(jnp.int32, (E * CP, TD), 0)

    def picks(r, marks):
        rank = jnp.sum(before * marks, axis=0, keepdims=True).astype(jnp.int32)
        back_x = x - lax.rem(r, NX)
        back_x = jnp.where(back_x < 0, back_x + NX, back_x)
        back_z = z - lax.div(r, NX)
        back_z = jnp.where(back_z < 0, back_z + NZ, back_z)
        turn = jnp.where(back_z <= NZ // 2, jnp.maximum(2 * back_z - 1, 0), 2 * (NZ - back_z))
        away = turn * NX + back_x
        return (slots == away * CP + rank).astype(F32)

    pick0 = picks(r0, marks0)
    pick1 = picks(r1, marks1)
    both = (pick0 + pick1).astype(BF)
    onehot[...] = both
    weight = jnp.sum(pick0 * rw_ref[0:1, :] + pick1 * rw_ref[1:2, :], axis=1, keepdims=True)
    row_in = dot(both, x_ref[...], 1, 0).astype(BF)
    row_cot = (weight * dot(both, cot_ref[...], 1, 0)).astype(BF)
    send1[:, :, 0:LANES] = row_in.reshape(E, CP, LANES)
    send1[:, :, LANES:] = row_cot.reshape(E, CP, LANES)
    recv1[0] = send1[0]

    mark("barrier")
    pl.semaphore_wait(barrier, SPN - 1 + NY - 1 + 1)

    def all_sent(src_of, dst_of, ss, rs, sign):
        def go(k):
            remote(src_of(k), dst_of(k), ss, rs, at_sp(sign * k)).start()

        def pair(k, carry):
            go(k)
            go(SPN - k)
            return carry

        lax.fori_loop(1, SPN // 2, pair, 0)
        go(SPN // 2)

    mark("p1send")
    def offsets(half):
        turns = range(NZ // 2) if half == 0 else range(NZ // 2, NZ)
        if NZ == 1:
            turns = ()
        for turn in reversed(turns):
            kz = (turn + 1) // 2 if turn % 2 or turn == 0 else NZ - turn // 2
            for kx in sorted(range(NX), key=lambda k: -min(k, NX - k)):
                if turn or kx:
                    yield turn * NX + kx, kz, kx

    def exchange(send, recv, ss, rs, half, sign):
        for at, kz, kx in offsets(half):
            to = lax.rem(z + sign * kz + NZ, NZ) * NX + lax.rem(x + sign * kx + NX, NX)
            remote(send.at[at], recv.at[at], ss, rs.at[half], (to, t)).start()

    def exchanged(recv, rs, half):
        first = 1 if half == 0 else EH
        if EH * (half + 1) > first:
            took(recv.at[pl.ds(first, EH * (half + 1) - first)], rs.at[half])

    for half in range(2):
        exchange(send1, recv1, p1_s, p1_r, half, -1)

    loads[4].wait()
    loads[5].wait()
    for j in range(NY):
        remote(
            wgu.at[pl.ds(pl.multiple_of(j * 256 + (1 - c) * LANES, LANES), LANES), :],
            wpart.at[j],
            wp_s,
            wp_r,
            partner,
        ).start()
    for load in loads[6:]:
        load.wait()

    mark("coef")
    decay_speed = jnp.log1p(jnp.exp(-dp_ref[...]))
    rate = jax.nn.sigmoid(rp_ref[...].astype(F32))
    inlet = jax.nn.sigmoid(ip_ref[...].astype(F32))
    signal = rv_ref[...].astype(F32)
    prev = ps_ref[...].astype(F32)
    log_decay = -decay_scale * rate * decay_speed
    decay = jnp.exp(log_decay)
    scale_in = jnp.sqrt(-expm1_neg(2.0 * log_decay))
    rec[...] = (decay * prev + scale_in * inlet * signal).astype(BF)
    gain = scale_in * inlet
    coef[0] = gain
    coef[1] = gain * signal * (1.0 - inlet)
    slope = decay * prev - inlet * signal * decay * decay / scale_in
    coef[2] = slope * (-decay_scale * decay_speed) * rate * (1.0 - rate)
    tok = lax.broadcasted_iota(jnp.int32, (TD, LANES), 0)
    span = jnp.where(tok < TD - 1, pltpu.roll(decay, TD - 1, 0), 1.0)
    n_levels = TD.bit_length() - 1
    for k in range(n_levels):
        inside = tok < TD - (1 << k)
        levels[k] = jnp.where(inside, span, 0.0)
        span = span * jnp.where(inside, pltpu.roll(span, TD - (1 << k), 0), 1.0)
    through[...] = span
    first_decay = decay[0:1, :]
    chs[0:1, :] = first_decay * span[0:1, :]

    half_i = lax.broadcasted_iota(jnp.int32, (RH, EH * CP), 0)
    half_j = lax.broadcasted_iota(jnp.int32, (RH, EH * CP), 1)
    slot_of = half_j & (CP - 1)
    dense = jnp.where(slot_of < CAP, (half_j >> 4) * CAP + slot_of, -1)
    sel = (half_i == dense).astype(BF)

    bufs = (inf, cotf)
    DIR = (1, -1)

    def hops(di, kind):
        return H if di == kind else H - 1

    def half_of(half):
        return pl.ds(half * RH, RH)

    def ring(half, kind, di, h):
        src = (-DIR[di] * h) % NY
        dst = (-DIR[di] * (h + 1)) % NY
        piece = half * 2 + kind
        return remote(
            bufs[kind].at[src, c, half_of(half), :],
            bufs[kind].at[dst, c, half_of(half), :],
            y_s.at[di, piece, h],
            y_r.at[di, piece, h],
            at_y(DIR[di]),
        )

    def across(half, kind, slot):
        ref = bufs[kind].at[slot, c, half_of(half), :]
        piece = half * 2 + kind
        return remote(ref, ref, d_s.at[piece, slot], d_r.at[piece, slot], partner)

    def y_at(j):
        return lax.rem(y + j, NY)

    def rows_at(j, wide):
        return pl.ds(pl.multiple_of(y_at(j) * wide, wide), wide)

    def at_distance(d):
        return sorted({d % NY, -d % NY})

    def begin(half):
        exchanged(recv1, p1_r, half)
        got = recv1[pl.ds(half * EH, EH)].reshape(EH * CP, 2 * LANES)
        kept = dot(sel, got, 1, 0).astype(BF)
        inf[0, c, half_of(half), :] = kept[:, :LANES]
        cotf[0, c, half_of(half), :] = kept[:, LANES:]
        for kind in range(2):
            for di in range(2):
                if hops(di, kind):
                    ring(half, kind, di, 0).start()
            across(half, kind, 0).start()

    def arrive(half, h):
        for kind in range(2):
            for di in range(2):
                if h <= hops(di, kind):
                    ring(half, kind, di, h - 1).wait_recv()
                    if h < hops(di, kind):
                        ring(half, kind, di, h).start()
                    across(half, kind, (-DIR[di] * h) % NY).start()

    def consume(half, d):
        for j in at_distance(d):
            at = half_of(half)
            across(half, 0, j).wait_recv()
            rows_in = jnp.concatenate([inf[j, 0, at, :], inf[j, 1, at, :]], axis=1)
            value = dot(rows_in, wgu[rows_at(j, 256), :], 1, 0)
            across(half, 1, j).wait_recv()
            rows_cot = jnp.concatenate([cotf[j, 0, at, :], cotf[j, 1, at, :]], axis=1)
            value_h = dot(rows_cot, dw[:, rows_at(j, 256)], 1, 1)
            if d:
                acc[at, :] += value
                hacc[at, :] += value_h
            else:
                acc[at, :] = value
                hacc[at, :] = value_h

    def swap(half):
        at = half_of(half)
        return remote(grads.at[at, :], grads_p.at[at, :], g_s.at[half], g_r.at[half], partner)

    def activate(half):
        at = half_of(half)
        gate_act = acc[at, :LANES]
        up_act = acc[at, LANES:]
        hidden_grad = hacc[at, :]
        squash = jax.nn.sigmoid(gate_act)
        silu_gate = gate_act * squash
        grads[at, :LANES] = (
            hidden_grad * up_act * squash * (1.0 + gate_act * (1.0 - squash))
        ).astype(BF)
        grads[at, LANES:] = (hidden_grad * silu_gate).astype(BF)
        swap(half).start()
        hid[at, :] = (silu_gate * up_act).astype(BF)

    ready = set()

    def need(half, j):
        if (half, j) in ready:
            return
        at = half_of(half)
        own = wgu[pl.ds(pl.multiple_of(y_at(j) * 256 + c * LANES, LANES), LANES), :]
        value = dot(grads[at, :], own, 1, 1)
        if not ready:
            took(wpart, wp_r)
        if not any(done == half for done, _ in ready):
            swap(half).wait_recv()
        ready.add((half, j))
        part[j, at, :] = value + dot(grads_p[at, :], wpart[y_at(j)], 1, 1)

    def chain(di, half, k):
        return remote(
            rss.at[di, half, k],
            rsr.at[di, half, k],
            q_s.at[di, half, k],
            q_r.at[di, half, k],
            at_y(DIR[di]),
        )

    def target(di, half, k):
        return (DIR[di] * (hops(di, half) - k)) % NY

    def pass_on(half, k):
        for di in (half, 1 - half):
            if k < hops(di, half):
                j = target(di, half, k)
                need(half, j)
                value = part[j, half_of(half), :]
                if k:
                    chain(di, half, k - 1).wait_recv()
                    value = value + rsr[di, half, k - 1].astype(F32)
                rss[di, half, k] = value.astype(BF)
                chain(di, half, k).start()

    def ahead(half, k):
        for di in (half, 1 - half):
            if k <= hops(di, half):
                need(half, target(di, half, k))

    def finish(half):
        need(half, 0)
        value = part[0, half_of(half), :]
        for di in (1 - half, half):
            n = hops(di, half)
            if n:
                chain(di, half, n - 1).wait_recv()
                value = value + rsr[di, half, n - 1].astype(F32)
        spread = dot(sel, value.astype(BF), 0, 0).astype(BF)
        send5[pl.ds(half * EH, EH)] = spread.reshape(EH, CP, LANES)
        if half == 0:
            recv5[0] = send5[0]
        exchange(send5, recv5, p5_s, p5_r, half, 1)

    def weight_grads(j):
        rows_in = jnp.concatenate([inf[j, 0], inf[j, 1]], axis=1)
        both = dot(rows_in, grads[...], 0, 0).astype(BF)
        gwg_ref[rows_at(j, 256), :] = both[:, :LANES]
        uwg_ref[rows_at(j, 256), :] = both[:, LANES:]
        rows_cot = jnp.concatenate([cotf[j, 0], cotf[j, 1]], axis=1)
        dwg_ref[:, rows_at(j, 256)] = dot(hid[...], rows_cot, 0, 0).astype(BF)

    mark("p1wait")
    begin(0)
    mark("p2")
    for i in range(1, H + 1):
        arrive(0, i)
        if i == 1:
            mark("p1waitB")
            begin(1)
            mark("p2B")
        else:
            arrive(1, i - 1)
        consume(0, i - 1)
        if i == H:
            consume(0, H)
            activate(0)
        if i >= 2:
            consume(1, i - 2)
    mark("p2last")
    arrive(1, H)
    consume(1, H - 1)
    mark("p4")
    pass_on(0, 0)
    consume(1, H)
    activate(1)
    ahead(0, 1)
    todo = list(range(NY))
    per = -(-NY // H)
    for k in range(H):
        if k + 1 < H:
            pass_on(0, k + 1)
        else:
            mark("finA")
            finish(0)
            mark("p4B")
        pass_on(1, k)
        if k + 2 <= H:
            ahead(0, k + 2)
        ahead(1, k + 1)
        for j in todo[:per]:
            weight_grads(j)
        todo = todo[per:]
    mark("finB")
    finish(1)
    mark("p5")
    for half in range(2):
        exchanged(recv5, p5_r, half)
    returned = dot(onehot[...], recv5[...].reshape(E * CP, LANES), 0, 0)
    mixf[0, c] = (returned + cot_ref[...].astype(F32)).astype(BF)

    mark("p6")
    TH = TD // 2
    staged = H == 4

    def mix_copy(src, dst, to, tokens):
        first, count = tokens
        at = pl.ds(first, count)
        n = dst * 2 + (first > 0)
        return remote(
            mixf.at[src % NY, c, at, :], mixf.at[dst % NY, c, at, :], m_s.at[n], m_r.at[n], at_y(to)
        )

    def mix_across(slot):
        ref = mixf.at[slot, c]
        return remote(ref, ref, md_s.at[slot], md_r.at[slot], partner)

    whole = (0, TD)
    if staged:
        direct = [2, NY - 2, 1, NY - 1]
    else:
        direct = [j for d in range(H, 0, -1) for j in at_distance(d)]
    mix_sends = []
    mix_recv = {}

    def mix_send(src, dst, to, tokens):
        copy = mix_copy(src, dst, to, tokens)
        mix_sends.append(copy)
        mix_recv.setdefault(dst, []).append(copy)
        return copy

    for j in direct:
        mix_send(0, -j % NY, j, whole).start()
    mix_across(0).start()
    passing = {}
    if staged:
        passing[NY - 2] = [
            mix_send(NY - 2, NY - 4, 2, (0, TH)),
            mix_send(NY - 2, NY - 3, 1, whole),
        ]
        passing[2] = [mix_send(2, 4, -2, (TH, TH)), mix_send(2, 3, -1, whole)]

    def mixer_chunk(j):
        if j:
            mix_across(j).wait_recv()
        else:
            mix_across(0).wait_recv()
        rows_mix = jnp.concatenate([mixf[j, 0], mixf[j, 1]], axis=1)
        outer = dot(rows_mix, rec[...], 0, 0).astype(BF)
        xsend[j] = outer.reshape(NX, 256 // NX, LANES)
        for dx in range(1, NX):
            to = lax.rem(x + dx, NX)
            remote(
                xsend.at[j, to], xrecv.at[j, dx], x_s, x_r.at[j], (z * NX + to, t)
            ).start()
        value = dot(rows_mix, op[:, rows_at(j, 256)], 1, 1)
        if j:
            sg[...] += value
        else:
            sg[...] = value

    def down_z(j):
        if NX > 1:
            took(xrecv.at[j, pl.ds(1, NX - 1)], x_r.at[j])
        total = xsend[j, x].astype(F32)
        for dx in range(1, NX):
            total = total + xrecv[j, dx].astype(F32)
        zsum[j] = total
        zsend[j] = total.astype(BF)
        to_z = y_at(j)
        dz = lax.rem(to_z - z + NZ, NZ)

        @pl.when(dz != 0)
        def _():
            remote(zsend.at[j], zrecv.at[dz], z_s, z_r, (to_z * NX + x, t)).start()

    order = [0]
    for d in range(1, H + 1):
        order += at_distance(d)
    if staged:
        waits = [2, NY - 2, 1, NY - 1, 3, NY - 3, 4]
    else:
        waits = order[1:]
    done = [0]
    for j in waits:
        for copy in mix_recv[j]:
            copy.wait_recv()
        for copy in passing.get(j, ()):
            copy.start()
        mix_across(j).start()
        mixer_chunk(done[-1])
        done.append(j)
    mixer_chunk(done[-1])

    mark("scan")
    local = sg[...]
    for k in range(n_levels):
        local = local + levels[k] * pltpu.roll(local, TD - (1 << k), 0)
    chs[1:2, :] = first_decay * local[0:1, :]
    all_sent(lambda k: chs, lambda k: chr_.at[k], c_s, c_r, -1)

    mark("xwait")
    for j in done:
        down_z(j)
    mine = zsum[lax.rem(z - y + NZ, NZ)]

    mark("cwait")
    took(chr_.at[pl.ds(1, SPN - 1)], c_r)
    entering = jnp.zeros((1, LANES), F32)
    for k in range(SPN - 1, 0, -1):
        entering = jnp.where(s + k < SPN, chr_[k, 1:2, :] + chr_[k, 0:1, :] * entering, entering)
    carried = local + through[...] * entering
    rvg_ref[...] = (carried * coef[0]).astype(BF)
    ipg_ref[...] = (carried * coef[1]).astype(BF)
    rpg_ref[...] = (carried * coef[2]).astype(BF)

    mark("zwait")
    took(zrecv.at[pl.ds(1, NZ - 1)], z_r)
    for dz in range(1, NZ):
        mine = mine + zrecv[dz].astype(F32)
    opg_ref[...] = mine

    mark("drain")
    took(recv1.at[pl.ds(1, SPN - 1)], p1_s)
    took(wpart, wp_s)
    for half in range(2):
        for di in range(2):
            for kind in range(2):
                for h in range(hops(di, kind)):
                    ring(half, kind, di, h).wait_send()
            for k in range(hops(di, half)):
                chain(di, half, k).wait_send()
        for kind in range(2):
            for j in range(NY):
                across(half, kind, j).wait_send()
        swap(half).wait_send()
    took(recv5.at[pl.ds(1, SPN - 1)], p5_s)
    for copy in mix_sends:
        copy.wait_send()
    for j in range(NY):
        mix_across(j).wait_send()
    if NX > 1:
        took(xrecv.at[:, pl.ds(1, NX - 1)], x_s)
    took(zrecv.at[pl.ds(1, NZ - 1)], z_s)
    took(chr_.at[pl.ds(1, SPN - 1)], c_s)
    mark(None)


def tail_kernel(*refs):
    copies = [
        pltpu.make_async_copy(refs[n], refs[7 + n], refs[14].at[n]) for n in range(7)
    ]
    for copy in copies:
        copy.start()
    for copy in copies:
        copy.wait()


def solution(mesh):
    SPN, TPN = mesh.shape["sp"], mesh.shape["tp"]
    NX = {32: 4, 8: 2, 4: 2}[SPN]
    NZ, NY = SPN // NX, TPN // 2

    def per_device(
        ffn_input,
        out_grad,
        routes,
        route_weight,
        gate_w,
        up_w,
        down_w,
        out_proj,
        rec_value,
        rate_pre,
        input_pre,
        prev_state,
        decay_param,
    ):
        TD, top = routes.shape
        E = SPN
        CAP = 5 * top * TD // (4 * E)
        R = E * CAP
        RH = R // 2
        D = gate_w.shape[1]
        H = NY // 2
        CP = SLOT_PAD
        vmem = pl.BlockSpec(memory_space=pltpu.VMEM)
        hbm = pl.BlockSpec(memory_space=pltpu.HBM)
        anywhere = pl.BlockSpec(memory_space=pl.ANY)
        dma = pltpu.SemaphoreType.DMA
        levels = TD.bit_length() - 1
        tile = pltpu.VMEM((TD, LANES), BF)
        scratch = [
            tile,
            tile,
            pltpu.VMEM((top, TD), jnp.int32),
            pltpu.VMEM((top, TD), F32),
            tile,
            tile,
            tile,
            tile,
            pltpu.VMEM((1, LANES), F32),
            pltpu.VMEM((D, 256), BF),
            pltpu.VMEM((NY, LANES, 256), BF),
            pltpu.VMEM((LANES, D), BF),
            pltpu.VMEM((LANES, D), BF),
            pltpu.VMEM((E * CP, TD), BF),
            pltpu.VMEM((E, CP, 256), BF),
            pltpu.VMEM((E, CP, 256), BF),
            pltpu.VMEM((NY, 2, R, LANES), BF),
            pltpu.VMEM((NY, 2, R, LANES), BF),
            pltpu.VMEM((R, 256), F32),
            pltpu.VMEM((R, LANES), F32),
            pltpu.VMEM((R, 256), BF),
            pltpu.VMEM((R, 256), BF),
            pltpu.VMEM((R, LANES), BF),
            pltpu.VMEM((NY, R, LANES), F32),
            pltpu.VMEM((2, 2, H, RH, LANES), BF),
            pltpu.VMEM((2, 2, H, RH, LANES), BF),
            pltpu.VMEM((E, CP, LANES), BF),
            pltpu.VMEM((E, CP, LANES), BF),
            pltpu.VMEM((NY, 2, TD, LANES), BF),
            pltpu.VMEM((TD, LANES), F32),
            pltpu.VMEM((levels, TD, LANES), F32),
            pltpu.VMEM((TD, LANES), F32),
            pltpu.VMEM((3, TD, LANES), F32),
            pltpu.VMEM((TD, LANES), BF),
            pltpu.VMEM((NY, NX, 256 // NX, LANES), BF),
            pltpu.VMEM((NY, NX, 256 // NX, LANES), BF),
            pltpu.VMEM((NZ, 256 // NX, LANES), F32),
            pltpu.VMEM((NZ, 256 // NX, LANES), BF),
            pltpu.VMEM((NZ, 256 // NX, LANES), BF),
            pltpu.VMEM((2, LANES), F32),
            pltpu.VMEM((SPN, 2, LANES), F32),
            dma((13,)),
            dma,
            dma,
            dma,
            dma((2,)),
            dma((2, 4, H)),
            dma((2, 4, H)),
            dma((4, NY)),
            dma((4, NY)),
            dma((2,)),
            dma((2,)),
            dma((2, 2, H)),
            dma((2, 2, H)),
            dma,
            dma((2,)),
            dma((2 * NY,)),
            dma((2 * NY,)),
            dma((NY,)),
            dma((NY,)),
            dma,
            dma((NY,)),
            dma,
            dma,
            dma,
            dma,
        ]
        shape = jax.ShapeDtypeStruct
        outs = pl.pallas_call(
            functools.partial(step_kernel, (SPN, NX, NY, E, CAP, TD, R)),
            out_shape=(
                shape((D, LANES), BF),
                shape((D, LANES), BF),
                shape((LANES, D), BF),
                shape((256 // NX, LANES), F32),
                shape((TD, LANES), BF),
                shape((TD, LANES), BF),
                shape((TD, LANES), BF),
            ),
            in_specs=[hbm] * 13,
            out_specs=[vmem] * 7,
            scratch_shapes=scratch,
            compiler_params=pltpu.CompilerParams(
                collective_id=0, has_side_effects=True, vmem_limit_bytes=24 * 1024 * 1024
            ),
        )(*[pltpu.with_memory_space_constraint(v, pltpu.HBM) for v in (
            ffn_input,
            out_grad,
            routes.T,
            route_weight.T,
            gate_w[0],
            up_w[0],
            down_w[0],
            out_proj,
            rec_value,
            rate_pre,
            input_pre,
            prev_state,
            decay_param.reshape(1, -1),
        )])
        outs = pl.pallas_call(
            tail_kernel,
            out_shape=tuple(shape(o.shape, o.dtype) for o in outs),
            in_specs=[anywhere] * 7,
            out_specs=[hbm] * 7,
            scratch_shapes=[dma((7,))],
            compiler_params=pltpu.CompilerParams(vmem_limit_bytes=1024 * 1024),
        )(*outs)
        return (outs[0][None], outs[1][None], outs[2][None], *outs[3:])

    tokens = P("sp", "tp")
    placed = (
        tokens,
        tokens,
        P("sp", None),
        P("sp", None),
        P("sp", None, "tp"),
        P("sp", None, "tp"),
        P("sp", "tp", None),
        P("tp", None),
        tokens,
        tokens,
        tokens,
        tokens,
        P("tp"),
    )
    return jax.shard_map(
        per_device,
        mesh=mesh,
        in_specs=placed,
        out_specs=(
            P("sp", None, "tp"),
            P("sp", None, "tp"),
            P("sp", "tp", None),
            tokens,
            tokens,
            tokens,
            tokens,
        ),
        check_vma=False,
    )
```

time: 99.6 us -> 87.1 us (0.87)
  local copies, waits for them, and re-layouts: 9.04 us -> 0 us
  Pallas kernels: 89.4 us -> 86.3 us
    unnamed x25 -> x0, local copies, waits for them, and re-layouts: 9.04 us -> none
    pallas_call x1, Pallas kernels: 89.4 us -> 85.1 us  [per_device(): pl.pallas_call(functools.partial(step_kernel, (SPN, NX, NY, E, CAP, TD, R...]
    pallas_call x0 -> x1, Pallas kernels: none -> 1.23 us  [per_device(): pl.pallas_call(tail_kernel, out_shape=tuple((shape(o.shape, o.dtype) for...]
where the time goes in v2:
time: 87.1 us; the launch traced here: 86.9 us
  Pallas kernels  86.3 us (99%)
    pallas_call x1, Pallas kernels, per_device(): pl.pallas_call(functools.partial(step_kernel, (SPN, NX, NY, E, CAP, TD, R...  85.1 us

profile of v2, /device:TPU:1, one launch (start us, length us, event | category | flops | bytes accessed | tf_op | source)
XLA Modules:
  0.0 86.9 jit_solution(5244867100704885526)
XLA Ops:
  0.6 85.1 %shard_map.180 = (bf16[2048,128]{1,0:T(8,128)(2,1)S(1)}, bf16[2048,128]{1,0:T(8,128)(2,1)S(1)}, bf16[128,2048]{1,0:T(8,128)(2,1)S(1)}, f32[64,128]{1,0:T(8,128)S...) custom-call(bf16[128,128]{1,0:T(8,128)(2,1)} %x_hbm.1, ...), custom_call_target="tpu_custom_call" | custom-call | tf_op jit(solution)/shard_map/pallas_call | solution.py:778
  85.7 1.2 %shard_map.181 = (bf16[2048,128]{1,0:T(8,128)(2,1)}, bf16[2048,128]{1,0:T(8,128)(2,1)}, bf16[128,2048]{1,0:T(8,128)(2,1)}, f32[64,128]{1,0:T(8,128)}, bf16[128,1...) custom-call(bf16[2048,128]{1,0:T(8,128)(2,1)S(1)} %get-tuple-element.21.refs_0_, ...), custom_call_target="tpu_custom_call" | custom-call | tf_op jit(solution)/shard_map/pallas_call | solution.py:810
